TPU v7x, 256 devices: a 4x2x16 block of a 4x16x16 slice. The times are simulated.
256 devices in a mesh: grp: 2 (over y), fs: 16 (over z), tp: 8 (over x, core).
Axes of the slice: x: 4, y: 2, z: 16, core: 2. Of those that a mesh axis runs over, the one named last changes fastest.
The devices are a block of a 4x16x16 slice.
Arguments:
- tokens: bfloat16 [32768, 2048], P(('grp', 'fs', 'tp')), parts along dimension 0, may hold values from -6 to 6
- mix_weight_in: bfloat16 [2048, 1024], P('fs', 'tp'), may hold values from -0.125 to 0.125
- pool_scale: float32 [1024], P('tp'), may hold values from 0.1 to 1.9
- mix_weight_out: bfloat16 [1024, 2048], P('tp', 'fs'), may hold values from -0.1875 to 0.1875
- up_weight: bfloat16 [2048, 8192], P('fs', 'tp'), may hold values from -0.125 to 0.125
- down_weight: bfloat16 [8192, 2048], P('tp', 'fs'), may hold values from -0.0625 to 0.0625
- gains: float32 [4, 2048], replicated, may hold values from 0.1 to 1.9
Outputs:
- result: bfloat16 [32768, 2048], P(('grp', 'fs', 'tp')), parts along dimension 0
There are 2 independent parts, one for each index of `grp`. A program takes and returns all parts, laid end to end along the dimension named above; an argument that names none is the same for every part. Nothing has to cross between parts.
All inputs are finite; a program needn't handle non-finite values.
Results may differ from a plain program's by a relative error of at most 0.02.
Values may be sent and summed in bfloat16 or wider, within the bound.
A program may use at most 64 MiB of HBM per device.

v0:
```python
import jax
import jax.numpy as jnp
from jax import lax
from jax.sharding import PartitionSpec as P

PW = 1024
GROUPS = 4


norm_eps = 1e-06
pool_spans = (2, 4, 8, 16)


def normalize(values, gain):
    upcast = values.astype(jnp.float32)
    return upcast * lax.rsqrt(jnp.mean(upcast * upcast, axis=-1, keepdims=True) + norm_eps) * gain


def pooling(mixed_in, first_channel):
    length = mixed_in.shape[0]
    upcast = mixed_in.astype(jnp.float32)
    running = jnp.cumsum(upcast, axis=0)
    position = jnp.arange(1, length + 1, dtype=jnp.float32)[:, None]
    channel = first_channel + jnp.arange(mixed_in.shape[1], dtype=jnp.int32)
    group_of = (channel // (PW // GROUPS))[None, :]
    average = jnp.zeros_like(upcast)
    for index, span in enumerate(pool_spans):
        lagged = jnp.pad(running, ((span, 0), (0, 0)))[:length]
        window_mean = (running - lagged) / jnp.minimum(position, float(span))
        average = jnp.where(group_of == index, window_mean, average)
    return average - upcast


def local(tokens, mix_weight_in, pool_scale, mix_weight_out, up_weight, down_weight, gains):
    normed = normalize(tokens, gains[0]).astype(jnp.bfloat16)
    gathered = lax.all_gather(normed, "tp", axis=0, tiled=True)
    mixed_acc = jnp.dot(
        gathered,
        lax.all_gather(mix_weight_in, "fs", axis=0, tiled=True),
        preferred_element_type=jnp.float32,
    )
    weight_out = lax.all_gather(mix_weight_out, "fs", axis=1, tiled=True)
    mixed_in = mixed_acc.astype(jnp.bfloat16)
    first_channel = lax.axis_index("tp") * mix_weight_in.shape[1]
    scaled = (pooling(mixed_in, first_channel) * pool_scale).astype(jnp.bfloat16)
    picked = scaled
    mixer_out = lax.psum_scatter(
        jnp.dot(picked, weight_out, preferred_element_type=jnp.float32).astype(jnp.bfloat16),
        "tp",
        scatter_dimension=0,
        tiled=True,
    )
    middle = (tokens.astype(jnp.float32) + normalize(mixer_out, gains[1])).astype(jnp.bfloat16)
    normed_two = normalize(middle, gains[2]).astype(jnp.bfloat16)
    gathered_two = lax.all_gather(normed_two, "tp", axis=0, tiled=True)
    whole_up = lax.all_gather(up_weight, "fs", axis=0, tiled=True)
    hidden_pre = jnp.dot(gathered_two, whole_up, preferred_element_type=jnp.float32)
    hidden_pre = jax.nn.relu(hidden_pre)
    squared = (hidden_pre * hidden_pre).astype(jnp.bfloat16)
    whole_down = lax.all_gather(down_weight, "fs", axis=1, tiled=True)
    picked = squared
    channel_out = lax.psum_scatter(
        jnp.dot(picked, whole_down, preferred_element_type=jnp.float32).astype(jnp.bfloat16),
        "tp",
        scatter_dimension=0,
        tiled=True,
    )
    return (middle.astype(jnp.float32) + normalize(channel_out, gains[3])).astype(jnp.bfloat16)


def solution(mesh):
    return jax.shard_map(
        local,
        mesh=mesh,
        in_specs=(
            P(("grp", "fs", "tp"), None),
            P("fs", "tp"),
            P("tp"),
            P("tp", "fs"),
            P("fs", "tp"),
            P("tp", "fs"),
            P(),
        ),
        out_specs=P(("grp", "fs", "tp"), None),
        check_vma=False,
    )
```

profile of v0, /device:TPU:33, one launch (start us, length us, event | category | flops | bytes accessed | tf_op | source)
XLA Modules:
  0.0 367.5 jit_solution(13481339233262587465)
XLA Ops:
  7.4 1.2 fusion.5
  8.6 1.0 fusion.48
  9.6 2.0 fusion.7
  11.7 0.1 reduce-scatter.3.cloned.1.call-start
  11.8 46.9 %all_gather.19 = bf16[2048,128]{1,0:T(8,128)(2,1)S(1)} all-gather(bf16[128,128]{1,0:T(8,128)(2,1)} %param.8), channel_id=1, replica_groups=mesh['grp'=2,'fs'=16,'tp'=8] {'fs'}, dimensions={0}, use_global_device_ids=true | all-gather | bytes 557056 | tf_op jit(solution)/shard_map/all_gather | solution.py:39
  58.7 22.9 %all_gather.20 = bf16[128,2048]{1,0:T(8,128)(2,1)S(1)} all-gather(bf16[128,128]{1,0:T(8,128)(2,1)} %param.10), channel_id=1, replica_groups=mesh['grp'=2,'fs'=16,'tp'=8] {'fs'}, dimensions={1}, use_global_device_ids=true | all-gather | bytes 557056 | tf_op jit(solution)/shard_map/all_gather | solution.py:42
  81.7 3.5 fusion
  85.1 0.3 fusion.27
  85.5 0.1 copy.9
  85.7 3.3 convolution_convert_fusion
  89.0 0.1 all-gather.9.cloned.1.call-start
  89.1 0.6 all-gather.9.cloned.1.call-update
  89.7 0.6 all-gather.11.cloned.1.call-update
  90.4 47.1 %reduce-scatter.3.cloned.1.call-done = bf16[128,2048]{1,0:T(8,128)(2,1)} async-done(((bf16[1024,2048]{1,0:T(8,128)(2,1)}), bf16[128,2048]{1,0:T(8,128)(2,1)}) %reduce-scatter.3.cloned.1.call-update) | async-done | bytes 524304 | tf_op jit(solution)/shard_map/reduce_scatter | solution.py:47
  137.5 1.2 fusion.1
  138.7 1.5 fusion.9
  140.2 1.0 fusion.11
  141.3 23.6 %all-gather.9.cloned.1.call-done = bf16[2048,1024]{1,0:T(8,128)(2,1)} async-done(((bf16[128,1024]{1,0:T(8,128)(2,1)}), bf16[2048,1024]{1,0:T(8,128)(2,1)}) %all-gather.9.cloned.1.call-update) | async-done | bytes 4194320 | tf_op jit(solution)/shard_map/all_gather | solution.py:56
  164.9 88.9 %all-gather.11.cloned.1.call-done = bf16[1024,2048]{1,0:T(8,128)(2,1)} async-done(((bf16[1024,128]{1,0:T(8,128)(2,1)}), bf16[1024,2048]{1,0:T(8,128)(2,1)}) %all-gather.11.cloned.1.call-update) | async-done | bytes 4194320 | tf_op jit(solution)/shard_map/all_gather | solution.py:60
  253.8 47.1 %all-gather.7.cloned.1.call-done = bf16[1024,2048]{1,0:T(8,128)(2,1)} async-done(((bf16[128,2048]{1,0:T(8,128)(2,1)}), bf16[1024,2048]{1,0:T(8,128)(2,1)}) %all-gather.7.cloned.1.call-update) | async-done | bytes 4194320 | tf_op jit(solution)/shard_map/all_gather | solution.py:55
  300.9 14.4 %convolution_convert_fusion.1 = bf16[1024,2048]{1,0:T(8,128)(2,1)} fusion(bf16[1024,2048]{1,0:T(8,128)(2,1)} %all-gather.11.cloned.1.call-done, bf16[1024,2048]{1,0:T(8,128)(2,1)} %all-gather.7.cloned.1.call-done, bf16[2048,1024]{1,0:T(8,128)(2,1)} %all-gather.9.cloned.1.call-done), kind=kOutput, calls=%fused_computation.2 | convolution fusion | flops 8595177472 | bytes 16777216 | tf_op jit(solution)/shard_map/dot_general | solution.py:63
  315.3 41.5 %reduce-scatter.5.cloned.1.call-done = bf16[128,2048]{1,0:T(8,128)(2,1)} async-done(((bf16[1024,2048]{1,0:T(8,128)(2,1)}), bf16[128,2048]{1,0:T(8,128)(2,1)}) %reduce-scatter.5.cloned.1.call-update) | async-done | bytes 524304 | tf_op jit(solution)/shard_map/reduce_scatter | solution.py:62
  356.8 1.2 fusion.3
  358.0 2.1 fusion.12
  (25 shorter events, 0.6 us)
Async XLA Ops:
  7.4 74.3 %all-gather.5.cloned.1.call-start = ((), (), s32[]{:S(2)}) async-start(), calls=%async_computation.2 | async-start | bytes 4718592 | tf_op jit(solution)/shard_map/all_gather | solution.py:36
  11.7 125.8 %reduce-scatter.3.cloned.1.call-start = ((), (), s32[]{:S(2)}) async-start(), calls=%async_computation.3 | async-start | bytes 4718592 | tf_op jit(solution)/shard_map/reduce_scatter | solution.py:47
  81.7 4.0 %copy-start.1 = (f32[128]{0:T(128)S(1)}, f32[128]{0:T(128)}, u32[]{:S(2)}) copy-start(f32[128]{0:T(128)} %param.9) | copy-start | bytes 1540
  89.0 49.8 %copy-start = (bf16[128,2048]{1,0:T(8,128)(2,1)S(1)}, bf16[128,2048]{1,0:T(8,128)(2,1)}, u32[]{:S(2)}) copy-start(bf16[128,2048]{1,0:T(8,128)(2,1)} %param.7) | copy-start | bytes 1572868
  89.0 75.9 %all-gather.9.cloned.1.call-start = ((), (), s32[]{:S(2)}) async-start(), calls=%async_computation.5 | async-start | bytes 4456448 | tf_op jit(solution)/shard_map/all_gather | solution.py:56
  89.7 164.1 %all-gather.11.cloned.1.call-start = ((), (), s32[]{:S(2)}) async-start(), calls=%async_computation.6 | async-start | bytes 4456448 | tf_op jit(solution)/shard_map/all_gather | solution.py:60
  90.3 210.6 %all-gather.7.cloned.1.call-start = ((), (), s32[]{:S(2)}) async-start(), calls=%async_computation.4 | async-start | bytes 4718592 | tf_op jit(solution)/shard_map/all_gather | solution.py:55
  141.2 215.5 %reduce-scatter.5.cloned.1.call-start = ((), (), s32[]{:S(2)}) async-start(), calls=%async_computation.7 | async-start | bytes 4718592 | tf_op jit(solution)/shard_map/reduce_scatter | solution.py:62
Sparse Core Ops, SparseCore 0:
  11.8 53.0 all-gather.4
  89.1 48.2 reduce-scatter.2
  315.4 41.3 reduce-scatter.4
Sparse Core Ops, SparseCore 1:
  91.3 73.6 all-gather.8
  166.5 87.2 all-gather.10
  255.6 45.3 all-gather.6
where the time goes:
time: 369 us; the launch traced here: 368 us
  waiting for transfers between devices  249 us (67%)
  blocking collectives  69.8 us (19%)
  matrix products  21.1 us (6%)
  between operations  14.9 us (4%)
  other arithmetic  10.7 us (3%)
    all_gather x1, waiting for transfers between devices, local(): whole_down = lax.all_gather(down_weight, 'fs', axis=1, tiled=True)  88.9 us
    reduce_scatter x1, waiting for transfers between devices, local(): lax.psum_scatter(jnp.dot(picked, weight_out, preferred_element_type=jnp.f...  47.1 us
    all_gather x1, waiting for transfers between devices, local(): gathered_two = lax.all_gather(normed_two, 'tp', axis=0, tiled=True)  47.1 us
    all_gather x1, blocking collectives, local(): lax.all_gather(mix_weight_in, 'fs', axis=0, tiled=True)  46.9 us
    reduce_scatter x1, waiting for transfers between devices, local(): lax.psum_scatter(jnp.dot(picked, whole_down, preferred_element_type=jnp.f...  41.5 us
    all_gather x1, waiting for transfers between devices, local(): whole_up = lax.all_gather(up_weight, 'fs', axis=0, tiled=True)  23.6 us
    all_gather x1, blocking collectives, local(): weight_out = lax.all_gather(mix_weight_out, 'fs', axis=1, tiled=True)  22.9 us
    dot_general x1, matrix products, local(): jnp.dot(picked, whole_down, preferred_element_type=jnp.float32)  14.4 us
  transfers between devices with their start and end apart: 6, of which 5 were waited for; matrix products, arithmetic and copies ran while one was open for 1% of the time, Pallas kernels for 0%

commit v1 on v0

v1 whole, which is shorter than its diff:
```python
import functools

import jax
import jax.numpy as jnp
from jax import lax
from jax.experimental import pallas as pl
from jax.experimental.pallas import tpu as pltpu
from jax.sharding import PartitionSpec as P

PW = 1024
GROUPS = 4
EPS = 1e-06
MESH = pl.DeviceIdType.MESH
F32 = jnp.float32
BF16 = jnp.bfloat16


def rms(v):
    return v * lax.rsqrt(jnp.mean(v * v, axis=-1, keepdims=True) + EPS)


class Copies:
    def __init__(self, send, recv):
        self.send, self.recv, self.sent = send, recv, []

    def make(self, slot, src, dst, where):
        return pltpu.make_async_remote_copy(
            src_ref=src,
            dst_ref=dst,
            send_sem=self.send.at[slot],
            recv_sem=self.recv.at[slot],
            device_id=where,
            device_id_type=MESH,
        )

    def start(self, slot, src, dst, where):
        copy = self.make(slot, src, dst, where)
        copy.start()
        self.sent.append(copy)

    def arrived(self, slot, dst, where):
        self.make(slot, dst, dst, where).wait_recv()

    def drain(self):
        for copy in self.sent:
            copy.wait_send()


class Ring:
    def __init__(self, copies, own, place, me, n, hops, ends, mirror=None):
        self.copies, self.own, self.place = copies, own, place
        self.me, self.n, self.hops, self.ends = me, n, hops, ends
        self.mirror = mirror

    def slot(self, way, hop):
        return (self.hops[0] if way else 0) + hop - 1

    def origin(self, way, hop):
        return lax.rem(self.me + (hop if way else self.n - hop), self.n)

    def begin(self):
        for way in (0, 1):
            if self.hops[way]:
                self.copies.start(
                    self.slot(way, 1), self.own, self.place(self.me), self.ends[way]
                )

    def event(self, hop):
        for way in (0, 1):
            if hop > self.hops[way]:
                continue
            block = self.place(self.origin(way, hop))
            self.copies.arrived(self.slot(way, hop), block, self.ends[way])
            if hop < self.hops[way]:
                self.copies.start(
                    self.slot(way, hop + 1), block, block, self.ends[way]
                )
            if self.mirror:
                copies, partner, _ = self.mirror
                copies.start(self.slot(way, hop), block, block, partner)

    def mirrored(self):
        if self.mirror:
            copies, partner, other = self.mirror
            for way in (0, 1):
                for hop in range(1, self.hops[way] + 1):
                    copies.arrived(
                        self.slot(way, hop), other(self.origin(way, hop)), partner
                    )


def kernel(
    sizes,
    tok, gain, scale, w_in, w_out, w_up, w_down,
    out,
    xg1, xg2, b_in, b_out, b_up, b_down, mixed, scaled, sq, mid,
    part1, part2, dd1, dd2, rel1, rel2, fin1, fin2, sum1, sum2,
    own_sem, *sems,
):
    n_fs, n_tp, paired = sizes
    grp, z, t = lax.axis_index("grp"), lax.axis_index("fs"), lax.axis_index("tp")
    chips = n_tp // 2
    x, core = t // 2, lax.rem(t, 2)
    parity = lax.rem(grp, 2)
    chip_r, chip_l = lax.rem(x + 1, chips), lax.rem(x + chips - 1, chips)
    chip_o = lax.rem(x + 2, chips)
    east, west = {"tp": chip_r * 2 + core}, {"tp": chip_l * 2 + core}
    mate = {"tp": x * 2 + 1 - core}
    up_z, down_z = {"fs": lax.rem(z + 1, n_fs)}, {"fs": lax.rem(z + n_fs - 1, n_fs)}
    twin = {"grp": grp + 1 - 2 * parity}
    rows, width = tok.shape
    half = rows // 2

    barrier = pltpu.get_barrier_semaphore()
    greeted = [east, west, mate, up_z, down_z] + ([twin] if paired else [])
    for where in greeted:
        pl.semaphore_signal(barrier, inc=1, device_id=where, device_id_type=MESH)

    pairs = [Copies(sems[2 * i], sems[2 * i + 1]) for i in range(len(sems) // 2)]
    c_in, c_out, c_uo, c_um, c_do, c_dm, c_uy, c_dy, c_ag1, c_ag2, c_rs1, c_rs2 = pairs

    k_in, k_up = w_in.shape[0], w_up.shape[0]
    n_out, n_down = w_out.shape[1], w_down.shape[1]
    f_down = w_down.shape[0]

    def rows_of(buffer, depth, first, size):
        return lambda o: buffer.at[
            pl.ds(pl.multiple_of(o * depth + first, 16), size), :
        ]

    def cols_of(buffer, depth, first, size):
        return lambda o: buffer.at[
            pl.ds(pl.multiple_of(first, 16), size),
            pl.ds(pl.multiple_of(o * depth, 128), depth),
        ]

    local = [
        pltpu.make_async_copy(w_in, rows_of(b_in, k_in, 0, k_in)(z), own_sem.at[0]),
        pltpu.make_async_copy(
            w_out, cols_of(b_out, n_out, 0, w_out.shape[0])(z), own_sem.at[1]
        ),
        pltpu.make_async_copy(w_up, rows_of(b_up, k_up, 0, k_up)(z), own_sem.at[2]),
        pltpu.make_async_copy(
            w_down, cols_of(b_down, n_down, 0, f_down)(z), own_sem.at[3]
        ),
    ]
    for copy in local:
        copy.start()

    big, small = n_fs // 2, n_fs - 1 - n_fs // 2
    ends = (up_z, down_z)
    if paired:
        outer_k, inner_k = 3 * k_up // 8, 2 * k_up // 8
        outer_f, inner_f = 3 * f_down // 8, 2 * f_down // 8
    else:
        outer_k, inner_k = k_up // 2, k_up // 2
        outer_f, inner_f = f_down // 2, f_down // 2

    def part_of(outer, inner):
        if paired:
            step = outer + inner
            return parity * step, outer, (1 - parity) * step
        return 0, inner, 0

    uo, um, uy = part_of(outer_k, inner_k)
    do, dm, dy = part_of(outer_f, inner_f)

    def own_rows(ref, first, size):
        return ref.at[pl.ds(pl.multiple_of(first, 16), size), :]

    ring = functools.partial(Ring, me=z, n=n_fs, ends=ends)
    r_in = ring(c_in, w_in, rows_of(b_in, k_in, 0, k_in), hops=(big, small))
    r_out = ring(
        c_out, w_out, cols_of(b_out, n_out, 0, w_out.shape[0]), hops=(small, big)
    )
    r_uo = ring(
        c_uo, own_rows(w_up, uo, outer_k), rows_of(b_up, k_up, uo, outer_k),
        hops=(big, small),
        mirror=(c_uy, twin, rows_of(b_up, k_up, uy, outer_k)) if paired else None,
    )
    r_um = ring(
        c_um, own_rows(w_up, um, inner_k), rows_of(b_up, k_up, um, inner_k),
        hops=(small, big),
    )
    r_do = ring(
        c_do, own_rows(w_down, do, outer_f), cols_of(b_down, n_down, do, outer_f),
        hops=(big, small),
        mirror=(c_dy, twin, cols_of(b_down, n_down, dy, outer_f)) if paired else None,
    )
    r_dm = ring(
        c_dm, own_rows(w_down, dm, inner_f), cols_of(b_down, n_down, dm, inner_f),
        hops=(small, big),
    )

    def mix_event(hop):
        r_in.event(hop)
        r_out.event(hop)

    def begin_down():
        r_do.begin()
        r_dm.begin()

    todo = []
    for hop in range(1, big + 1):
        todo.append(functools.partial(mix_event, hop))
        todo.append(functools.partial((r_uo, r_um)[(hop - 1) % 2].event, (hop + 1) // 2))
    reached = (big + 1) // 2
    todo.append(begin_down)
    lag = reached
    for hop in range(reached + 1, big + 1):
        todo += [functools.partial(r_uo.event, hop), functools.partial(r_um.event, hop)]
        todo += [functools.partial(r_do.event, hop - lag), functools.partial(r_dm.event, hop - lag)]
    for hop in range(big - lag + 1, big + 1):
        todo += [functools.partial(r_do.event, hop), functools.partial(r_dm.event, hop)]

    def pump(count):
        for _ in range(count):
            if todo:
                todo.pop(0)()

    def block(buffer, tp, part=None):
        first, size = (0, rows) if part is None else (part * half, half)
        return buffer.at[pl.ds(pl.multiple_of(tp * rows + first, 16), size), :]

    t_w, t_e, t_o = chip_l * 2 + core, chip_r * 2 + core, chip_o * 2 + core
    flip = 1 - 2 * core

    class Gather:
        def __init__(self, copies, buffer):
            self.c, self.b = copies, buffer

        def begin(self):
            c, b = self.c, self.b
            c.start(0, block(b, t, 0), block(b, t, 0), east)
            c.start(3, block(b, t, 1), block(b, t, 1), west)
            c.start(1, block(b, t, 1), block(b, t, 1), east)
            c.start(4, block(b, t, 0), block(b, t, 0), west)
            c.start(6, block(b, t), block(b, t), mate)

        def got_mate(self):
            self.c.arrived(6, block(self.b, t + flip), mate)

        def got(self, slot, tp, part, where, relay=None):
            c, piece = self.c, block(self.b, tp, part)
            c.arrived(slot, piece, where)
            if relay is not None:
                c.start(relay, piece, piece, east if relay == 2 else west)
            c.start(7 + slot, piece, piece, mate)

        def first(self):
            self.got(0, t_w, 0, west, 2)
            self.got(3, t_e, 1, east, 5)

        def second(self):
            self.got(1, t_w, 1, west)
            self.got(4, t_e, 0, east)

        def third(self):
            self.got(2, t_o, 0, west)
            self.got(5, t_o, 1, east)

        def mates_near(self):
            for slot, tp, part in ((0, t_w, 0), (3, t_e, 1), (1, t_w, 1), (4, t_e, 0)):
                self.c.arrived(7 + slot, block(self.b, tp + flip, part), mate)

        def mates_far(self):
            for slot, part in ((2, 0), (5, 1)):
                self.c.arrived(7 + slot, block(self.b, t_o + flip, part), mate)

    dest = (chip_o, chip_r, chip_l, x)

    def lines(count, body, step=16):
        @pl.loop(0, count // step)
        def _(i):
            body(pl.ds(pl.multiple_of(i * step, step), step))

    class Sum:
        def __init__(self, copies, part, dd, rel, fin, total):
            self.c, self.part, self.dd = copies, part, dd
            self.rel, self.fin, self.total = rel, fin, total

        def give(self, i):
            self.c.start(
                i, block(self.part, dest[i] * 2 + 1 - core), self.dd.at[i], mate
            )

        def add(self, i):
            self.c.arrived(i, self.dd.at[i], mate)
            base = (dest[i] * 2 + core) * rows

            def body(at):
                mine = self.part[pl.ds(pl.multiple_of(base + at.start, 16), 16), :]
                both = mine.astype(F32) + self.dd[i, at, :].astype(F32)
                self.total[i, at, :] = both.astype(BF16)

            lines(rows, body)

        def half_of(self, i, h):
            return self.total.at[i, pl.ds(h * half, half), :]

        def far(self):
            self.add(0)
            self.c.start(4, self.half_of(0, 0), self.rel.at[0], east)
            self.c.start(5, self.half_of(0, 1), self.rel.at[1], west)

        def near(self):
            self.add(1)
            self.c.start(
                6, self.half_of(1, 1), self.fin.at[0, pl.ds(half, half), :], east
            )
            self.add(2)
            self.c.start(
                7, self.half_of(2, 0), self.fin.at[1, pl.ds(0, half), :], west
            )

        def relay(self):
            for way, i, h, where, back in ((0, 1, 0, east, west), (1, 2, 1, west, east)):
                self.c.arrived(4 + way, self.rel.at[way], back)

                def body(at):
                    to = pl.ds(pl.multiple_of(h * half + at.start, 16), 16)
                    both = self.total[i, to, :].astype(F32) + self.rel[way, at, :].astype(F32)
                    self.total[i, to, :] = both.astype(BF16)

                lines(half, body)
                self.c.start(
                    8 + way,
                    self.half_of(i, h),
                    self.fin.at[way, pl.ds(h * half, half), :],
                    where,
                )

        def own(self):
            self.c.arrived(3, self.dd.at[3], mate)

        def final_near(self):
            self.c.arrived(6, self.fin.at[0, pl.ds(half, half), :], west)
            self.c.arrived(7, self.fin.at[1, pl.ds(0, half), :], east)

        def final(self):
            self.c.arrived(8, self.fin.at[0, pl.ds(0, half), :], west)
            self.c.arrived(9, self.fin.at[1, pl.ds(half, half), :], east)

        def result(self, at):
            mine = self.part[pl.ds(pl.multiple_of(t * rows + at.start, 16), 16), :]
            total = mine.astype(F32) + self.dd[3, at, :].astype(F32)
            total += self.fin[0, at, :].astype(F32)
            total += self.fin[1, at, :].astype(F32)
            return total.astype(BF16).astype(F32)

    g1, g2 = Gather(c_ag1, xg1), Gather(c_ag2, xg2)
    s1 = Sum(c_rs1, part1, dd1, rel1, fin1, sum1)
    s2 = Sum(c_rs2, part2, dd2, rel2, fin2, sum2)

    def gain_row(i):
        return gain[pl.ds(i, 1), :]

    def first_norm(at):
        y = rms(tok[at, :].astype(F32)) * gain_row(0)
        xg1[pl.ds(pl.multiple_of(t * rows + at.start, 16), 16), :] = y.astype(BF16)

    lines(rows, first_norm)
    mixed[pl.ds(0, 16), :] = jnp.zeros((16, mixed.shape[1]), F32)

    pl.semaphore_wait(barrier, len(greeted))
    r_in.begin()
    r_out.begin()
    g1.begin()
    r_uo.begin()
    r_um.begin()
    for copy in local:
        copy.wait()

    pair = 2 * rows

    def chip_rows(chip):
        return pl.ds(pl.multiple_of(chip * pair, 16), pair)

    pump(2)
    g1.got_mate()
    pump(2)
    g1.first()
    pump(4)
    g1.second()
    pump(2)
    g1.mates_near()
    g1.third()
    pump(4)
    g1.mates_far()
    pump(2 * big - 14)

    @pl.loop(0, chips)
    def _(i):
        y = jnp.dot(xg1[chip_rows(i), :], b_in[...], preferred_element_type=F32)
        mixed[pl.ds(pl.multiple_of(i * pair + 16, 16), pair), :] = y.astype(BF16).astype(F32)

    channels = mixed.shape[1]
    lane = lax.broadcasted_iota(jnp.int32, (1, channels), 1)
    group = (t * channels + lane) // (PW // GROUPS)
    span = jnp.where(group == 0, 2, jnp.where(group == 1, 4, jnp.where(group == 2, 8, 16)))

    @pl.loop(0, n_tp)
    def _(i):
        v = mixed[pl.ds(pl.multiple_of(i * rows, 16), rows + 16), :]
        two = v + pltpu.roll(v, 1, 0)
        four = two + pltpu.roll(two, 2, 0)
        eight = four + pltpu.roll(four, 4, 0)
        sixteen = eight + pltpu.roll(eight, 8, 0)
        total = jnp.where(group == 0, two, jnp.where(group == 1, four, jnp.where(group == 2, eight, sixteen)))
        total, v = total[16:, :], v[16:, :]
        position = i * rows + 1 + lax.broadcasted_iota(jnp.int32, (rows, channels), 0)
        count = jnp.minimum(position, span).astype(F32)
        y = (total / count - v) * scale[...]
        scaled[pl.ds(pl.multiple_of(i * rows, 16), rows), :] = y.astype(BF16)

    tile = 256

    def mix_back(chip):
        @pl.loop(0, width // tile)
        def _(j):
            at = pl.ds(pl.multiple_of(j * tile, tile), tile)
            y = jnp.dot(scaled[chip_rows(chip), :], b_out[:, at], preferred_element_type=F32)
            part1[chip_rows(chip), at] = y.astype(BF16)

    mix_back(chip_o)
    s1.give(0)
    mix_back(chip_r)
    s1.give(1)
    s1.far()
    mix_back(chip_l)
    s1.give(2)
    s1.near()
    mix_back(x)
    s1.give(3)
    pump(4)
    s1.relay()
    s1.own()
    pump(4)
    s1.final_near()
    pump(3)
    s1.final()

    def second_norm(at):
        m = tok[at, :].astype(F32) + rms(s1.result(at)) * gain_row(1)
        m = m.astype(BF16)
        mid[at, :] = m
        y = rms(m.astype(F32)) * gain_row(2)
        xg2[pl.ds(pl.multiple_of(t * rows + at.start, 16), 16), :] = y.astype(BF16)

    lines(rows, second_norm)
    g2.begin()
    pump(4)
    g2.got_mate()
    g2.first()
    pump(3)
    g2.second()
    g2.mates_near()
    pump(3)

    def expand(chip):
        @pl.loop(0, sq.shape[1] // tile)
        def _(j):
            at = pl.ds(pl.multiple_of(j * tile, tile), tile)
            h = jnp.dot(xg2[chip_rows(chip), :], b_up[:, at], preferred_element_type=F32)
            h = jnp.maximum(h, 0.0)
            sq[chip_rows(chip), at] = (h * h).astype(BF16)

    def contract(chip):
        @pl.loop(0, width // tile)
        def _(j):
            at = pl.ds(pl.multiple_of(j * tile, tile), tile)
            y = jnp.dot(sq[chip_rows(chip), :], b_down[:, at], preferred_element_type=F32)
            part2[chip_rows(chip), at] = y.astype(BF16)

    g2.third()
    r_uo.mirrored()
    expand(x)
    pump(2)
    expand(chip_l)
    pump(2)
    expand(chip_r)
    g2.mates_far()
    pump(2)
    expand(chip_o)
    pump(len(todo))
    r_do.mirrored()

    contract(chip_o)
    s2.give(0)
    contract(chip_r)
    s2.give(1)
    s2.far()
    contract(chip_l)
    s2.give(2)
    s2.near()
    contract(x)
    s2.give(3)
    s2.relay()
    s2.own()
    s2.final_near()
    s2.final()

    def last_norm(at):
        y = mid[at, :].astype(F32) + rms(s2.result(at)) * gain_row(3)
        out[at, :] = y.astype(BF16)

    lines(rows, last_norm)
    for copies in pairs:
        copies.drain()


def solution(mesh):
    n_fs, n_tp = mesh.shape["fs"], mesh.shape["tp"]
    paired = mesh.shape["grp"] % 2 == 0

    def layer(tokens, mix_in, pool_scale, mix_out, up, down, gains):
        rows, width = tokens.shape
        channels, hidden = mix_in.shape[1], up.shape[1]
        seq = rows * n_tp
        vmem = pl.BlockSpec(memory_space=pltpu.VMEM)
        far = pl.BlockSpec(memory_space=pl.ANY)
        sems = []
        for count in [n_fs - 1] * 8 + [13, 13, 10, 10]:
            sems += [pltpu.SemaphoreType.DMA((count,))] * 2
        sums = lambda *lead: pltpu.VMEM((*lead, width), BF16)
        return pl.pallas_call(
            functools.partial(kernel, (n_fs, n_tp, paired)),
            out_shape=jax.ShapeDtypeStruct((rows, width), BF16),
            in_specs=[vmem, vmem, vmem, far, far, far, far],
            out_specs=vmem,
            scratch_shapes=[
                sums(seq), sums(seq),
                pltpu.VMEM((width, channels), BF16),
                sums(channels),
                pltpu.VMEM((width, hidden), BF16),
                sums(hidden),
                pltpu.VMEM((seq + 16, channels), F32),
                pltpu.VMEM((seq, channels), BF16),
                pltpu.VMEM((seq, hidden), BF16),
                sums(rows),
                sums(seq), sums(seq),
                sums(4, rows), sums(4, rows),
                sums(2, rows // 2), sums(2, rows // 2),
                sums(2, rows), sums(2, rows),
                sums(3, rows), sums(3, rows),
                pltpu.SemaphoreType.DMA((4,)),
                *sems,
            ],
            compiler_params=pltpu.CompilerParams(
                collective_id=0,
                has_side_effects=True,
                vmem_limit_bytes=60 * 1024 * 1024,
            ),
            name="layer",
        )(tokens, gains, pool_scale.reshape(1, -1), mix_in, mix_out, up, down)

    spread = P(("grp", "fs", "tp"), None)
    return jax.shard_map(
        layer,
        mesh=mesh,
        in_specs=(
            spread,
            P("fs", "tp"),
            P("tp"),
            P("tp", "fs"),
            P("fs", "tp"),
            P("tp", "fs"),
            P(),
        ),
        out_specs=spread,
        check_vma=False,
    )
```

time: 369 us -> 147 us (0.40)
  waiting for transfers between devices: 249 us -> 0 us
  Pallas kernels: 0 us -> 145 us
  blocking collectives: 69.8 us -> 0 us
  matrix products: 21.1 us -> 0 us
  between operations: 14.9 us -> 0.01 us
  other arithmetic: 10.7 us -> 0 us
    all_gather x4 -> x0, waiting for transfers between devices: 160 us -> none  [the longest x1 88.9 us: local(): whole_down = lax.all_gather(down_weight, 'fs', axis=1, tiled=True)]
    pallas_call x0 -> x1, Pallas kernels: none -> 145 us  [layer(): pl.pallas_call(functools.partial(kernel, (n_fs, n_tp, paired)), out_shape...]
    reduce_scatter x2 -> x0, waiting for transfers between devices: 88.6 us -> none  [the longest x1 47.1 us: local(): lax.psum_scatter(jnp.dot(picked, weight_out, preferred_element_type=jnp.f...]
    all_gather x2 -> x0, blocking collectives: 69.8 us -> none  [the longest x1 46.9 us: local(): lax.all_gather(mix_weight_in, 'fs', axis=0, tiled=True)]
    dot_general x3 -> x0, matrix products: 21.1 us -> none  [the longest x1 14.4 us: local(): jnp.dot(picked, whole_down, preferred_element_type=jnp.float32)]
    reduce_sum x4 -> x0, other arithmetic: 5.14 us -> none  [normalize(): jnp.mean(upcast * upcast, axis=-1, keepdims=True) + norm_eps]
    convert_element_type x3 -> x0, other arithmetic: 5.13 us -> none  [the longest x1 2.11 us: local(): (middle.astype(jnp.float32) + normalize(channel_out, gains[3])).astype(jn...]
  transfers between devices with their start and end apart: 6 -> 0, of which waited for: 5 -> 0; matrix products, arithmetic and copies ran while one was open for 1% -> 0% of each run, Pallas kernels for 0% -> 0%
where the time goes in v1:
time: 147 us
  Pallas kernels  145 us (99%)
  local copies, waits for them, and re-layouts  1.88 us (1%)
    pallas_call x1, Pallas kernels, layer(): pl.pallas_call(functools.partial(kernel, (n_fs, n_tp, paired)), out_shape...  145 us

profile of v1, /device:TPU:33, one launch (start us, length us, event | category | flops | bytes accessed | tf_op | source)
XLA Modules:
  0.0 146.5 jit_solution(5454797283015373172)
XLA Ops:
  0.0 144.6 %layer.1 = bf16[128,2048]{1,0:T(8,128)(2,1)} custom-call(bf16[128,2048]{1,0:T(8,128)(2,1)} %tok.1, f32[4,2048]{1,0:T(4,128)} %gain.1, f32[1,128]{1,0:T(1,128)} %bitcast.1, bf16[128,128]{1,0:T(8,128)(2,1)} %w_in.1, bf16[128,128]{1,0:T(8,128)(2,1)} %w_out.1, bf16[128,1024]{1,0:T(8,128)(2,1)} %w_up.1, bf16[1024,128]{1,0:T(8,128)(2,1)} %w_down.1), custom_call_target="tpu_custom_call" | custom-call | tf_op jit(solution)/shard_map/layer/pallas_call | solution.py:526
  144.6 1.9 %copy.9 = bf16[128,2048]{1,0:T(8,128)(2,1)} copy(bf16[128,2048]{1,0:T(8,128)(2,1)} %layer.1) | data formatting | bytes 1048576

commit v2 on v0

v2 whole, which is shorter than its diff:
```python
import contextlib
import functools
import math

import jax
import jax.numpy as jnp
from jax import lax
from jax.experimental import pallas as pl
from jax.experimental.pallas import tpu as pltpu
from jax.sharding import PartitionSpec as P

PW = 1024
GROUPS = 4
EPS = 1e-06
CUTS = (4, 6)
MIX_TIMES = (9.0, 12.5, 16.0, 20.0)
UO_BEGIN, UM_BEGIN, DOWN_BEGIN, MIX_DONE = 4.2, 9.2, 24.7, 24.9
UO_TIMES = (16.5, 22.5, 28.2, 33.5, 38.6, 43.6, 49.8, 53.5)
UM_TIMES = (18.0, 24.0, 29.6, 34.5, 39.4, 44.4, 50.5, 54.3)
DOWN_TIMES = (34.8, 44.8, 52.5, 57.5, 62.5, 66.8, 70.9, 73.9)
LAST_TIMES = (
    (68.8, 69.5, 70.2, 71.0, 71.8, 77.6),
    (73.0, 73.5, 74.0, 74.5, 75.4, 80.1),
    (79.5, 79.7, 79.8, 79.9, 80.0, 82.5),
)
MESH = pl.DeviceIdType.MESH
F32 = jnp.float32
BF16 = jnp.bfloat16


def scope(name):
    return contextlib.nullcontext()


def rms(v):
    return v * lax.rsqrt(jnp.mean(v * v, axis=-1, keepdims=True) + EPS)


class Copies:
    def __init__(self, name, send, recv, spare):
        self.name, self.send, self.recv, self.spare = name, send, recv, spare
        self.together = recv.shape[0] == 1
        self.begun, self.size = set(), 0

    def make(self, slot, src, dst, where):
        return pltpu.make_async_remote_copy(
            src_ref=src,
            dst_ref=dst,
            send_sem=self.send.at[0],
            recv_sem=self.recv.at[0 if self.together else slot],
            device_id=where,
            device_id_type=MESH,
        )

    def start(self, slot, src, dst, where):
        self.make(slot, src, dst, where).start()
        self.begun.add(slot)
        self.size += math.prod(src.shape)

    def arrived(self, slot, dst, where):
        assert slot in self.begun, (self.name, slot)
        with scope(f"{self.name}_{slot}"):
            self.make(slot, dst, dst, where).wait_recv()

    def all_of(self):
        for ref in self.spare:
            lines, rest = divmod(self.size, ref.shape[1])
            if rest == 0 and lines % 16 == 0 and lines <= ref.shape[0]:
                return ref.at[pl.ds(0, lines), :]
        raise ValueError(self.name)

    def arrived_all(self, where):
        with scope(f"{self.name}_all"):
            every = self.all_of()
            self.make(0, every, every, where).wait_recv()

    def drain(self, where):
        every = self.all_of()
        self.make(0, every, every, where).wait_send()


class Ring:
    def __init__(self, copies, own, place, me, n, hops, ends, mirror=None):
        self.copies, self.own, self.place = copies, own, place
        self.me, self.n, self.hops, self.ends = me, n, hops, ends
        self.mirror = mirror

    def slot(self, way, hop):
        return (self.hops[0] if way else 0) + hop - 1

    def block(self, way, hop):
        step = hop if way else self.n - hop
        return self.place(lax.rem(self.me + step, self.n))

    def send(self, way, hop, src, dst, reach=1):
        if hop <= self.hops[way]:
            where = self.ends[reach - 1][way]
            self.copies.start(self.slot(way, hop), src, dst, where)

    def take(self, way, hop, reach=1):
        block = self.block(way, hop)
        self.copies.arrived(self.slot(way, hop), block, self.ends[reach - 1][way])
        return block

    def onward(self, way, hop, block):
        return block

    def reflect(self, way, hop, block):
        if self.mirror:
            copies, partner = self.mirror
            copies.start(self.slot(way, hop), block, block, partner)

    def begin(self):
        for way in (0, 1):
            self.send(way, 1, self.own, self.onward(way, 1, self.place(self.me)))

    def event(self, hop, later=False):
        for way in (0, 1):
            if hop <= self.hops[way]:
                block = self.take(way, hop)
                self.send(way, hop + 1, block, self.onward(way, hop + 1, block))
                if not later:
                    self.reflect(way, hop, block)

    def reflect_both(self, hop):
        for way in (0, 1):
            if hop <= self.hops[way]:
                self.reflect(way, hop, self.block(way, hop))

    def mirrored(self):
        if self.mirror:
            copies, partner = self.mirror
            assert len(copies.begun) == sum(self.hops)
            copies.arrived_all(partner)


class Arrivals(Ring):
    def __init__(self, *args, cuts=None):
        super().__init__(*args)
        self.cuts = (*cuts, self.n)

    def block(self, way, hop):
        return self.place(min(2 * hop - 1 + way, self.n - 1))

    def onward(self, way, hop, block):
        return self.block(way, hop) if hop <= self.hops[way] else block

    def group(self, hop):
        return sum(hop > cut for cut in self.cuts)

    def reflect(self, way, hop, block):
        if self.mirror:
            copies, partner = self.mirror
            copies = copies[self.group(hop)]
            copies.start(self.slot(way, hop), block, block, partner)

    def mirrored(self, group):
        if self.mirror:
            copies, partner = self.mirror
            hops = [h for way in (0, 1) for h in range(1, self.hops[way] + 1)]
            count = sum(self.group(h) == group for h in hops)
            assert len(copies[group].begun) == count
            copies[group].arrived_all(partner)


class Leaps(Ring):
    def begin(self):
        for way in (0, 1):
            self.send(way, 2, self.own, self.place(self.me), 2)
        for way in (0, 1):
            self.send(way, 1, self.own, self.place(self.me))

    def event(self, leap):
        hop = 2 * leap
        blocks = [None, None]
        for way in (0, 1):
            if hop <= self.hops[way]:
                blocks[way] = self.take(way, hop, 2)
                self.send(way, hop + 2, blocks[way], blocks[way], 2)
        for way in (0, 1):
            if blocks[way] is not None:
                self.send(way, hop + 1, blocks[way], blocks[way])
                self.reflect(way, hop, blocks[way])
        for way in (0, 1):
            if hop - 1 <= self.hops[way]:
                self.reflect(way, hop - 1, self.take(way, hop - 1))


def lines(first, count, body, step=16, unroll=4):
    @pl.loop(0, count // step, unroll=unroll)
    def _(i):
        body(pl.ds(pl.multiple_of(first + i * step, step), step))


class Gather:
    def __init__(self, copies, buffer, rows, place):
        self.c, self.buffer, self.rows = copies, buffer, rows
        self.t, self.t_w, self.t_e, self.t_o, self.flip = place[:5]
        self.east, self.west, self.mate = place[5:]

    def piece(self, tp, first, size):
        unit = self.rows // 4
        start = pl.multiple_of(tp * self.rows + first * unit, 16)
        return self.buffer.at[pl.ds(start, size * unit), :]

    def begin(self, h):
        for k, way in ((0, 0), (1, 1), (1, 0), (0, 1)):
            q = 2 * h + k
            piece = self.piece(self.t, q, 1)
            self.c.start(4 * way + q, piece, piece, self.west if way else self.east)
        piece = self.piece(self.t, 2 * h, 2)
        self.c.start(12 + h, piece, piece, self.mate)

    def take(self, slot, tp, q, way):
        where = self.east if way else self.west
        self.c.arrived(slot, self.piece(tp, q, 1), where)

    def hand(self, slot, tp, h):
        piece = self.piece(tp, 2 * h, 2)
        self.c.start(slot, piece, piece, self.mate)

    def near(self, h):
        for way, tp, k in ((0, self.t_w, 0), (1, self.t_e, 1)):
            q = 2 * h + k
            self.take(4 * way + q, tp, q, way)
            piece = self.piece(tp, q, 1)
            self.c.start(
                8 + 2 * way + h, piece, piece, self.west if way else self.east
            )
        for way, tp, k in ((0, self.t_w, 1), (1, self.t_e, 0)):
            q = 2 * h + k
            self.take(4 * way + q, tp, q, way)
            self.hand(14 + 2 * way + h, tp, h)

    def far(self, h):
        for way in (0, 1):
            self.take(8 + 2 * way + h, self.t_o, 2 * h + way, way)
        self.hand(18 + h, self.t_o, h)

    def from_mate(self, slot, tp, h):
        self.c.arrived(slot, self.piece(tp + self.flip, 2 * h, 2), self.mate)

    def mate_own(self):
        for h in (0, 1):
            self.from_mate(12 + h, self.t, h)

    def mate_near(self):
        for way, tp in ((0, self.t_w), (1, self.t_e)):
            for h in (0, 1):
                self.from_mate(14 + 2 * way + h, tp, h)

    def mate_far(self):
        for h in (0, 1):
            self.from_mate(18 + h, self.t_o, h)


class Sum:
    def __init__(self, copies, bufs, rows, dest, core, ways, cols):
        self.c, self.rows, self.dest, self.core = copies, rows, dest, core
        self.part, self.dd, self.rel, self.fin, self.total = bufs
        self.east, self.west, self.mate = ways
        self.unit, self.cols = rows // 4, cols

    def base(self, i, core):
        return (self.dest[i] * 2 + core) * self.rows

    def give(self, i):
        start = pl.multiple_of(self.base(i, 1 - self.core), 16)
        piece = self.part.at[pl.ds(start, self.rows), self.cols]
        self.c.start(i, piece, self.dd.at[i, :, self.cols], self.mate)

    def add(self, i):
        self.c.arrived(i, self.dd.at[i, :, self.cols], self.mate)
        base, cols = self.base(i, self.core), self.cols

        def body(at):
            mine = self.part[pl.ds(pl.multiple_of(base + at.start, 16), 16), cols]
            both = mine.astype(F32) + self.dd[i, at, cols].astype(F32)
            self.total[i, at, cols] = both.astype(BF16)

        lines(0, self.rows, body)

    def quarter(self, ref, i, q):
        return ref.at[i, pl.ds(q * self.unit, self.unit), self.cols]

    def far(self, way):
        for k in (0, 1):
            self.c.start(
                4 + 2 * way + k,
                self.quarter(self.total, 0, 2 * k + way),
                self.quarter(self.rel, way, k),
                self.west if way else self.east,
            )

    def direct(self, way):
        for k in (0, 1):
            q = 2 * k + 1 - way
            self.c.start(
                8 + 2 * way + k,
                self.quarter(self.total, 1 + way, q),
                self.quarter(self.fin, way, q),
                self.west if way else self.east,
            )

    def relay(self, way, k):
        there, back = (self.west, self.east) if way else (self.east, self.west)
        self.c.arrived(4 + 2 * way + k, self.quarter(self.rel, way, k), back)
        q, cols = 2 * k + way, self.cols
        shift = (q - k) * self.unit

        def body(at):
            to = pl.ds(pl.multiple_of(at.start + shift, 16), 16)
            both = self.total[1 + way, to, cols].astype(F32)
            both += self.rel[way, at, cols].astype(F32)
            self.total[1 + way, to, cols] = both.astype(BF16)

        lines(k * self.unit, self.unit, body)
        self.c.start(
            12 + 2 * way + k,
            self.quarter(self.total, 1 + way, q),
            self.quarter(self.fin, way, q),
            there,
        )

    def own(self):
        self.c.arrived(3, self.dd.at[3, :, self.cols], self.mate)

    def finish(self, h):
        for slot, way, q in (
            (8 + h, 0, 2 * h + 1),
            (10 + h, 1, 2 * h),
            (12 + h, 0, 2 * h),
            (14 + h, 1, 2 * h + 1),
        ):
            back = self.east if way else self.west
            self.c.arrived(slot, self.quarter(self.fin, way, q), back)

    def result(self, at):
        base = self.base(3, self.core)
        mine = self.part[pl.ds(pl.multiple_of(base + at.start, 16), 16), :]
        total = mine.astype(F32) + self.dd[3, at, :].astype(F32)
        total += self.fin[0, at, :].astype(F32)
        total += self.fin[1, at, :].astype(F32)
        return total.astype(BF16).astype(F32)


NAMES = ("in", "out", "iy", "oy", "uo", "um", "uy", "do", "dm", "dx", "dy", "dz", "ag", "ah", "rs", "rt", "ru", "rv")


def kernel(
    sizes,
    tokens, gain, scale, w_in, w_out, w_up, w_down,
    out,
    tok, xg1, xg2, b_in, b_out, b_up, b_down, mixed, scaled, sq, mid, last,
    part1, part2, dd1, dd2, rel1, rel2, fin1, fin2, sum1, sum2,
    own_sem, *sems,
):
    n_fs, n_tp, paired = sizes
    grp, z, t = lax.axis_index("grp"), lax.axis_index("fs"), lax.axis_index("tp")
    chips = n_tp // 2
    x, core = t // 2, lax.rem(t, 2)
    parity = lax.rem(grp, 2)
    chip_r, chip_l = lax.rem(x + 1, chips), lax.rem(x + chips - 1, chips)
    chip_o = lax.rem(x + 2, chips)
    east, west = {"tp": chip_r * 2 + core}, {"tp": chip_l * 2 + core}
    mate = {"tp": x * 2 + 1 - core}
    ends = tuple(
        tuple({"fs": lax.rem(z + d, n_fs)} for d in (k, n_fs - k)) for k in (1, 2)
    )
    twin = {"grp": grp + 1 - 2 * parity}
    rows, width = tok.shape
    half = rows // 2

    barrier = pltpu.get_barrier_semaphore()
    greeted = [east, west, mate, *ends[0], *ends[1]] + ([twin] if paired else [])
    for where in greeted:
        pl.semaphore_signal(barrier, inc=1, device_id=where, device_id_type=MESH)

    spare = (xg1, b_up, b_in)
    pairs = [Copies(n, sems[2 * i], sems[2 * i + 1], spare) for i, n in enumerate(NAMES)]
    c_in, c_out, c_iy, c_oy, c_uo, c_um, c_uy, c_do, c_dm = pairs[:9]
    c_dys, (c_ag1, c_ag2, c_rs1), c_last = pairs[9:12], pairs[12:15], pairs[15:]

    k_in, k_up, k_out = w_in.shape[0], w_up.shape[0], w_out.shape[0]
    n_out, n_down, f_down = w_out.shape[1], w_down.shape[1], w_down.shape[0]

    def rows_of(buffer, depth, first, size):
        return lambda o: buffer.at[
            pl.ds(pl.multiple_of(o * depth + first, 16), size), :
        ]

    def cols_of(buffer, depth, first, size):
        return lambda o: buffer.at[
            pl.ds(pl.multiple_of(first, 16), size),
            pl.ds(pl.multiple_of(o * depth, 128), depth),
        ]

    fetch = pltpu.make_async_copy(tokens, tok, own_sem.at[4])
    fetch.start()

    big, small = n_fs // 2, n_fs - 1 - n_fs // 2

    def make(kind, copies, shard, of, buffer, depth, first, size, hops, mirror):
        own = shard.at[pl.ds(pl.multiple_of(first, 16), size), :]
        place = of(buffer, depth, first, size)
        if mirror is not None:
            mirror = (mirror[0], twin)
        return kind(copies, own, place, z, n_fs, hops, ends, mirror)

    def split(depth, eighths):
        if not paired:
            return (0, depth // 2), (depth // 2, depth // 2), None
        outer = eighths * depth // 8
        inner = depth - 2 * outer
        skip = outer + inner
        return (parity * skip, outer), (outer, inner), (1 - parity) * skip

    def halves(depth):
        if not paired:
            return 0, depth, None
        return parity * (depth // 2), depth // 2, (1 - parity) * (depth // 2)

    def mirror(copies, first):
        return None if first is None else (copies, first)

    far_e, far_w = (big, small), (small, big)
    f, size, m = halves(k_in)
    r_in = make(Leaps, c_in, w_in, rows_of, b_in, k_in, f, size, far_e, mirror(c_iy, m))
    f, size, m = halves(k_out)
    r_out = make(Leaps, c_out, w_out, cols_of, b_out, n_out, f, size, far_w, mirror(c_oy, m))
    outer, inner, m = split(k_up, 3)
    r_uo = make(Ring, c_uo, w_up, rows_of, b_up, k_up, *outer, far_e, mirror(c_uy, m))
    r_um = make(Ring, c_um, w_up, rows_of, b_up, k_up, *inner, far_w, None)
    outer, inner, m = split(f_down, 2)
    kind = functools.partial(Arrivals, cuts=CUTS)
    r_do = make(kind, c_do, w_down, cols_of, b_down, n_down, *outer, far_e, mirror(c_dys, m))
    r_dm = make(kind, c_dm, w_down, cols_of, b_down, n_down, *inner, far_w, None)

    due = []

    def at_time(when, *steps):
        for step in steps:
            due.append((when, len(due), step))

    step = functools.partial

    def due_at(times, k):
        if k < len(times):
            return times[k]
        return times[-1] + (k + 1 - len(times)) * (times[-1] - times[-2])

    for leap in range((big + 1) // 2):
        at_time(due_at(MIX_TIMES, leap), step(r_in.event, leap + 1), step(r_out.event, leap + 1))
    at_time(UO_BEGIN, r_uo.begin)
    at_time(UM_BEGIN, r_um.begin)
    at_time(DOWN_BEGIN, r_do.begin, r_dm.begin)
    for hop in range(1, big + 1):
        when = due_at(UO_TIMES, hop - 1)
        at_time(when, step(r_uo.event, hop, when < MIX_DONE))
        if when < MIX_DONE:
            at_time(MIX_DONE, step(r_uo.reflect_both, hop))
        at_time(due_at(UM_TIMES, hop - 1), step(r_um.event, hop))
        when = due_at(DOWN_TIMES, hop - 1)
        at_time(when, step(r_do.event, hop))
        at_time(when + 0.4, step(r_dm.event, hop))

    ways = (east, west, mate)
    place = (t, chip_l * 2 + core, chip_r * 2 + core, chip_o * 2 + core, 1 - 2 * core)
    dest = (chip_o, chip_r, chip_l, x)
    g1 = Gather(c_ag1, xg1, rows, place + ways)
    g2 = Gather(c_ag2, xg2, rows, place + ways)
    s1 = Sum(c_rs1, (part1, dd1, rel1, fin1, sum1), rows, dest, core, ways, pl.ds(0, width))
    bufs = (part2, dd2, rel2, fin2, sum2)
    bounds = [0] + [(2 * cut + 1) * n_down for cut in CUTS] + [width]
    lasts = [
        Sum(copies, bufs, rows, dest, core, ways, pl.ds(low, high - low))
        for copies, low, high in zip(c_last, bounds, bounds[1:])
    ]

    def gain_row(i):
        return gain[pl.ds(i, 1), :]

    def first_norm(at):
        y = rms(tok[at, :].astype(F32)) * gain_row(0)
        xg1[pl.ds(pl.multiple_of(t * rows + at.start, 16), 16), :] = y.astype(BF16)

    with scope("barrier"):
        pl.semaphore_wait(barrier, len(greeted))
    r_in.begin()
    r_out.begin()
    with scope("fetch"):
        fetch.wait()
    with scope("norm0"):
        lines(0, half, first_norm)
    g1.begin(0)
    lines(half, half, first_norm)
    g1.begin(1)
    local = [
        pltpu.make_async_copy(w_in, rows_of(b_in, k_in, 0, k_in)(z), own_sem.at[0]),
        pltpu.make_async_copy(w_out, cols_of(b_out, n_out, 0, k_out)(z), own_sem.at[1]),
        pltpu.make_async_copy(w_up, rows_of(b_up, k_up, 0, k_up)(z), own_sem.at[2]),
        pltpu.make_async_copy(w_down, cols_of(b_down, n_down, 0, f_down)(0), own_sem.at[3]),
    ]
    for copy in local:
        copy.start()
    mixed[pl.ds(0, 16), :] = jnp.zeros((16, mixed.shape[1]), F32)

    pair = 2 * rows

    def chip_rows(chip):
        return pl.ds(pl.multiple_of(chip * pair, 16), pair)

    def rows_at(tp):
        return pl.ds(pl.multiple_of(tp * rows, 16), rows)

    def mix(chip):
        y = jnp.dot(xg1[chip_rows(chip), :], b_in[...], preferred_element_type=F32)
        mixed[pl.ds(pl.multiple_of(chip * pair + 16, 16), pair), :] = y.astype(BF16).astype(F32)

    channels = mixed.shape[1]
    lane = lax.broadcasted_iota(jnp.int32, (1, channels), 1)
    group = (t * channels + lane) // (PW // GROUPS)

    def pick(a, b, c, d):
        return jnp.where(group == 0, a, jnp.where(group == 1, b, jnp.where(group == 2, c, d)))

    span = pick(2, 4, 8, 16)

    def pool(chip):
        for part in (0, 1):
            first = (chip * 2 + part) * rows
            v = mixed[pl.ds(pl.multiple_of(first, 16), rows + 16), :]
            two = v + pltpu.roll(v, 1, 0)
            four = two + pltpu.roll(two, 2, 0)
            eight = four + pltpu.roll(four, 4, 0)
            total = pick(two, four, eight, eight + pltpu.roll(eight, 8, 0))
            total, v = total[16:, :], v[16:, :]
            position = first + 1 + lax.broadcasted_iota(jnp.int32, (rows, channels), 0)
            count = jnp.minimum(position, span).astype(F32)
            y = (total / count - v) * scale[...]
            scaled[rows_at(chip * 2 + part), :] = y.astype(BF16)

    every = pl.ds(0, width)

    def product(left, right, to, at, cols=every, finish=lambda y: y):
        y = jnp.dot(left[at, :], right[:, cols], preferred_element_type=F32)
        to[at, cols] = finish(y).astype(BF16)

    def for_mate(total, left, right, i):
        product(left, right, total.part, rows_at(dest[i] * 2 + 1 - core), total.cols)
        total.give(i)

    def for_me(total, left, right, i):
        product(left, right, total.part, rows_at(dest[i] * 2 + core), total.cols)

    def expand(chip):
        def finish(h):
            h = jnp.maximum(h, 0.0)
            return h * h

        product(xg2, b_up, sq, chip_rows(chip), pl.ds(0, sq.shape[1]), finish)

    def second_norm(at):
        m = tok[at, :].astype(F32) + rms(s1.result(at)) * gain_row(1)
        m = m.astype(BF16)
        mid[at, :] = m
        y = rms(m.astype(F32)) * gain_row(2)
        xg2[pl.ds(pl.multiple_of(t * rows + at.start, 16), 16), :] = y.astype(BF16)

    def middle(h):
        s1.finish(h)
        with scope("norm1"):
            lines(h * half, half, second_norm)
        g2.begin(h)

    def weights_in():
        for copy in local:
            copy.wait()
        r_in.mirrored()
        r_out.mirrored()

    do = functools.partial
    back = (scaled, b_out)
    at_time(12.8, do(g1.near, 0))
    at_time(18.5, do(g1.near, 1))
    at_time(21.5, do(g1.far, 0))
    at_time(24.5, do(g1.far, 1))
    at_time(25.0, weights_in, g1.mate_own, do(mix, x), g1.mate_near, do(mix, chip_r))
    at_time(26.0, do(pool, chip_r), do(for_mate, s1, *back, 1), do(for_me, s1, *back, 1))
    at_time(26.5, do(mix, chip_l), g1.mate_far, do(mix, chip_o), do(pool, chip_o))
    at_time(26.8, do(s1.add, 1), do(s1.direct, 0), do(for_mate, s1, *back, 0))
    at_time(27.5, do(pool, chip_l), do(for_mate, s1, *back, 2), do(for_me, s1, *back, 0))
    at_time(28.0, do(s1.add, 0), do(s1.far, 1), do(s1.far, 0))
    at_time(28.5, do(for_me, s1, *back, 2), do(s1.add, 2), do(s1.direct, 1))
    at_time(29.5, do(pool, x), do(for_mate, s1, *back, 3))
    at_time(30.5, do(for_me, s1, *back, 3))
    at_time(36.2, do(s1.relay, 1, 0))
    at_time(36.4, do(s1.relay, 0, 0), s1.own)
    at_time(38.7, do(s1.relay, 1, 1))
    at_time(39.2, do(s1.relay, 0, 1))
    at_time(46.5, do(middle, 0))
    at_time(49.0, do(middle, 1))
    at_time(56.0, g2.mate_own, do(g2.near, 0))
    at_time(61.5, do(g2.near, 1))
    at_time(62.5, r_uo.mirrored, do(expand, x))
    at_time(63.5, g2.mate_near, do(expand, chip_r))
    at_time(64.5, do(g2.far, 0), do(expand, chip_l))
    at_time(67.0, do(g2.far, 1))
    at_time(68.5, g2.mate_far, do(expand, chip_o))
    back = (sq, b_down)

    for turn, s in enumerate(lasts):
        first, second, third, fourth, fifth, sixth = LAST_TIMES[turn]
        at_time(first, do(r_do.mirrored, turn), do(for_mate, s, *back, 1))
        at_time(first, do(for_me, s, *back, 1), do(for_mate, s, *back, 2))
        at_time(second, do(s.add, 1), do(s.direct, 0), do(for_me, s, *back, 2))
        at_time(third, do(for_mate, s, *back, 0), do(s.add, 2), do(s.direct, 1))
        at_time(fourth, do(for_me, s, *back, 0), do(s.add, 0), do(s.far, 0), do(s.far, 1))
        at_time(fifth, do(for_mate, s, *back, 3), do(for_me, s, *back, 3))
        for k in (0, 1):
            at_time(sixth + 1.5 * k, do(s.relay, 0, k), do(s.relay, 1, k))
    for _, _, step in sorted(due, key=lambda entry: entry[:2]):
        step()
    for s in lasts:
        s.own()
    with scope("drain"):
        for copies in pairs[: -len(lasts)]:
            if copies.size:
                copies.drain(mate)

    def last_norm(at):
        total = lasts[0].result(at)
        scaled_by = lax.rsqrt(jnp.mean(total * total, axis=-1, keepdims=True) + EPS)
        for slot in range(n_fs):
            away = (slot + 1) // 2
            origin = lax.rem(z + (n_fs - away if slot % 2 else away), n_fs)
            cols = pl.ds(pl.multiple_of(origin * n_down, 128), n_down)
            y = total[:, slot * n_down : (slot + 1) * n_down] * scaled_by
            y = mid[at, cols].astype(F32) + y * gain[pl.ds(3, 1), cols]
            last[at, cols] = y.astype(BF16)

    puts = []
    for h in (0, 1):
        for s in lasts:
            s.finish(h)
        with scope("norm3"):
            lines(h * half, half, last_norm)
        at = pl.ds(h * half, half)
        puts.append(pltpu.make_async_copy(last.at[at, :], out.at[at, :], own_sem.at[h]))
        puts[-1].start()
    with scope("end"):
        for copies in c_last:
            copies.drain(mate)
        for put in puts:
            put.wait()


def solution(mesh):
    n_fs, n_tp = mesh.shape["fs"], mesh.shape["tp"]
    paired = mesh.shape["grp"] % 2 == 0

    def layer(tokens, mix_in, pool_scale, mix_out, up, down, gains):
        rows, width = tokens.shape
        channels, hidden = mix_in.shape[1], up.shape[1]
        seq = rows * n_tp
        vmem = pl.BlockSpec(memory_space=pltpu.VMEM)
        far = pl.BlockSpec(memory_space=pl.ANY)
        sems = []
        counts = {"iy": 1, "oy": 1, "uy": 1, "dx": 1, "dy": 1, "dz": 1, "ag": 20, "ah": 20, "rs": 16, "rt": 16, "ru": 16, "rv": 16}
        for name in NAMES:
            sems.append(pltpu.SemaphoreType.DMA((1,)))
            sems.append(pltpu.SemaphoreType.DMA((counts.get(name, n_fs - 1),)))
        sums = lambda *lead: pltpu.VMEM((*lead, width), BF16)
        return pl.pallas_call(
            functools.partial(kernel, (n_fs, n_tp, paired)),
            out_shape=jax.ShapeDtypeStruct((rows, width), BF16),
            in_specs=[far, vmem, vmem, vmem, vmem, far, far],
            out_specs=far,
            scratch_shapes=[
                sums(rows),
                sums(seq), sums(seq),
                pltpu.VMEM((width, channels), BF16),
                sums(channels),
                pltpu.VMEM((width, hidden), BF16),
                sums(hidden),
                pltpu.VMEM((seq + 16, channels), F32),
                pltpu.VMEM((seq, channels), BF16),
                pltpu.VMEM((seq, hidden), BF16),
                sums(rows), sums(rows),
                sums(seq), sums(seq),
                sums(4, rows), sums(4, rows),
                sums(2, rows // 2), sums(2, rows // 2),
                sums(2, rows), sums(2, rows),
                sums(3, rows), sums(3, rows),
                pltpu.SemaphoreType.DMA((5,)),
                *sems,
            ],
            compiler_params=pltpu.CompilerParams(
                collective_id=0,
                has_side_effects=True,
                vmem_limit_bytes=60 * 1024 * 1024,
            ),
            name="layer",
        )(tokens, gains, pool_scale.reshape(1, -1), mix_in, mix_out, up, down)

    spread = P(("grp", "fs", "tp"), None)
    return jax.shard_map(
        layer,
        mesh=mesh,
        in_specs=(
            spread,
            P("fs", "tp"),
            P("tp"),
            P("tp", "fs"),
            P("fs", "tp"),
            P("tp", "fs"),
            P(),
        ),
        out_specs=spread,
        check_vma=False,
    )
```

time: 369 us -> 124 us (0.34)
  waiting for transfers between devices: 249 us -> 0 us
  Pallas kernels: 0 us -> 122 us
  blocking collectives: 69.8 us -> 0 us
  matrix products: 21.1 us -> 0 us
  between operations: 14.9 us -> 0.01 us
  other arithmetic: 10.7 us -> 0 us
    all_gather x4 -> x0, waiting for transfers between devices: 160 us -> none  [the longest x1 88.9 us: local(): whole_down = lax.all_gather(down_weight, 'fs', axis=1, tiled=True)]
    pallas_call x0 -> x1, Pallas kernels: none -> 122 us  [layer(): pl.pallas_call(functools.partial(kernel, (n_fs, n_tp, paired)), out_shape...]
    reduce_scatter x2 -> x0, waiting for transfers between devices: 88.6 us -> none  [the longest x1 47.1 us: local(): lax.psum_scatter(jnp.dot(picked, weight_out, preferred_element_type=jnp.f...]
    all_gather x2 -> x0, blocking collectives: 69.8 us -> none  [the longest x1 46.9 us: local(): lax.all_gather(mix_weight_in, 'fs', axis=0, tiled=True)]
    dot_general x3 -> x0, matrix products: 21.1 us -> none  [the longest x1 14.4 us: local(): jnp.dot(picked, whole_down, preferred_element_type=jnp.float32)]
    reduce_sum x4 -> x0, other arithmetic: 5.14 us -> none  [normalize(): jnp.mean(upcast * upcast, axis=-1, keepdims=True) + norm_eps]
    convert_element_type x3 -> x0, other arithmetic: 5.13 us -> none  [the longest x1 2.11 us: local(): (middle.astype(jnp.float32) + normalize(channel_out, gains[3])).astype(jn...]
  transfers between devices with their start and end apart: 6 -> 0, of which waited for: 5 -> 0; matrix products, arithmetic and copies ran while one was open for 1% -> 0% of each run, Pallas kernels for 0% -> 0%
where the time goes in v2:
time: 124 us
  Pallas kernels  122 us (98%)
  local copies, waits for them, and re-layouts  1.88 us (2%)
    pallas_call x1, Pallas kernels, layer(): pl.pallas_call(functools.partial(kernel, (n_fs, n_tp, paired)), out_shape...  122 us

profile of v2, /device:TPU:33, one launch (start us, length us, event | category | flops | bytes accessed | tf_op | source)
XLA Modules:
  0.0 123.8 jit_solution(6436823564231478958)
XLA Ops:
  0.0 121.9 %layer.1 = bf16[128,2048]{1,0:T(8,128)(2,1)} custom-call(bf16[128,2048]{1,0:T(8,128)(2,1)} %tokens.1, f32[4,2048]{1,0:T(4,128)} %gain.1, f32[1,128]{1,0:T(1,128)} %bitcast.1, bf16[128,128]{1,0:T(8,128)(2,1)} %w_in.1, bf16[128,128]{1,0:T(8,128)(2,1)} %w_out.1, bf16[128,1024]{1,0:T(8,128)(2,1)} %w_up.1, bf16[1024,128]{1,0:T(8,128)(2,1)} %w_down.1), custom_call_target="tpu_custom_call" | custom-call | tf_op jit(solution)/shard_map/layer/pallas_call | solution.py:674
  121.9 1.9 %copy.9 = bf16[128,2048]{1,0:T(8,128)(2,1)} copy(bf16[128,2048]{1,0:T(8,128)(2,1)} %layer.1) | data formatting | bytes 1048576
